TPU v7x, 32 devices: a whole 2x2x4 slice. The times are simulated.
32 devices in a mesh: grp: 2 (over y), sp: 4 (over z), tp: 4 (over x, core).
Axes of the slice: x: 2, y: 2, z: 4, core: 2. Of those that a mesh axis runs over, the one named last changes fastest.
Arguments:
- residual: bfloat16 [2048, 2048], P(('grp', 'sp', 'tp')), parts along dimension 0, may hold values from -6 to 6
- query_nope: bfloat16 [2048, 1024], P(('grp', 'sp'), 'tp'), parts along dimension 0, may hold values from -6 to 6
- query_rope: bfloat16 [2048, 512], P(('grp', 'sp'), 'tp'), parts along dimension 0, may hold values from -240 to 240
- kv_latent: bfloat16 [2048, 256], P(('grp', 'sp')), parts along dimension 0, may hold values from -6 to 6
- rope_key: bfloat16 [2048, 64], P(('grp', 'sp')), parts along dimension 0, may hold values from -6 to 6
- latent_gain: float32 [256], replicated, may hold values from 0.1 to 1.9
- w_key: bfloat16 [256, 1024], P(None, 'tp'), may hold values from -0.375 to 0.375
- w_value: bfloat16 [256, 1024], P(None, 'tp'), may hold values from -0.375 to 0.375
- w_out: bfloat16 [1024, 2048], P('tp'), may hold values from -0.1875 to 0.1875
- post_gain: float32 [2048], replicated, may hold values from 0.1 to 1.9
- routes: int32 [2048, 2], P(('grp', 'sp', 'tp')), parts along dimension 0, may hold values from 0 to 3, all different within a row; in each aligned block of 64 rows (0 to 63, 64 to 127, ...) at most 48 rows name the same one
- route_weight: float32 [2048, 2], P(('grp', 'sp', 'tp')), parts along dimension 0, may hold values from 0.25 to 1
- moe_gain: float32 [2048], replicated, may hold values from 0.1 to 1.9
- w_gate: bfloat16 [4, 2048, 3584], P('sp', None, 'tp'), may hold values from -0.125 to 0.125
- w_up: bfloat16 [4, 2048, 3584], P('sp', None, 'tp'), may hold values from -0.125 to 0.125
- w_down: bfloat16 [4, 3584, 2048], P('sp', 'tp'), may hold values from -0.09375 to 0.09375
Outputs:
- mixed: bfloat16 [2048, 2048], P(('grp', 'sp', 'tp')), parts along dimension 0
There are 2 independent parts, one for each index of `grp`. A program takes and returns all parts, laid end to end along the dimension named above; an argument that names none is the same for every part. Nothing has to cross between parts.
Inputs may be any that keep to these rules, and one draw needn't show every extreme that they name: `routes`: each row names two different experts. Among the 64 rows of one device no expert is named more than 48 times, and some device names some expert exactly 48 times.
All inputs are finite; a program needn't handle non-finite values.
Results may differ from a plain program's by a relative error of at most 0.014.
Values may be sent and summed in bfloat16 or wider, within the bound.
A program may use at most 128 MiB of HBM per device.

v0:
```python
import jax
import jax.numpy as jnp
from jax import lax
from jax.sharding import PartitionSpec as P

HEADS = 8
NOPE = 128
ROPE = 64
VDIM = 128


epsilon = 1e-06
rope_base = 10000.0


def rms_scale(inputs, gain_vector):
    mean_square = jnp.mean(inputs * inputs, axis=-1, keepdims=True)
    return inputs * lax.rsqrt(mean_square + epsilon) * gain_vector


def tables(positions, rot_width):
    frequency = 1.0 / rope_base ** (jnp.arange(0, rot_width, 2, dtype=jnp.float32) / rot_width)
    angles = positions.astype(jnp.float32)[:, None] * frequency[None, :]
    return (jnp.cos(angles), jnp.sin(angles))


def rotate(inputs, cosine_table, sine_table):
    half_width = inputs.shape[-1] // 2
    first_half = inputs[..., :half_width]
    second_half = inputs[..., half_width:]
    return jnp.concatenate(
        [
            first_half * cosine_table - second_half * sine_table,
            second_half * cosine_table + first_half * sine_table,
        ],
        axis=-1,
    )


def expand(latent_rows, rope_rows, latent_gain, w_key, w_value):
    normed = rms_scale(latent_rows.astype(jnp.float32), latent_gain).astype(jnp.bfloat16)
    key_plain = jnp.dot(normed, w_key, preferred_element_type=jnp.float32).astype(jnp.bfloat16)
    value_plain = jnp.dot(normed, w_value, preferred_element_type=jnp.float32).astype(jnp.bfloat16)
    key_positions = jnp.arange(latent_rows.shape[0], dtype=jnp.int32)
    cosine_table, sine_table = tables(key_positions, rope_rows.shape[1])
    key_turned = rotate(rope_rows.astype(jnp.float32), cosine_table, sine_table).astype(
        jnp.bfloat16
    )
    return (key_plain, value_plain, key_turned)


def body(
    residual,
    query_nope,
    query_rope,
    kv_latent,
    rope_key,
    latent_gain,
    w_key,
    w_value,
    w_out,
    post_gain,
    routes,
    route_weight,
    moe_gain,
    w_gate,
    w_up,
    w_down,
):
    tok_rows = query_nope.shape[0]
    heads_here = HEADS // lax.axis_size("tp")
    first_row = lax.axis_index("sp") * tok_rows
    last_row = first_row + tok_rows - 1
    positions = first_row + jnp.arange(tok_rows, dtype=jnp.int32)
    cosine_table, sine_table = tables(positions, ROPE)
    query_plain = query_nope.reshape(tok_rows, heads_here, NOPE)
    query_turned = rotate(
        query_rope.reshape(tok_rows, heads_here, ROPE).astype(jnp.float32),
        cosine_table[:, None, :],
        sine_table[:, None, :],
    ).astype(jnp.bfloat16)
    score_scale = (NOPE + ROPE) ** (-0.5)

    def update(state_now, key_plain, value_plain, key_turned):
        row_max, row_sum, running = state_now
        key_count = key_plain.shape[0]
        key_heads = key_plain.reshape(key_count, heads_here, NOPE)
        value_heads = value_plain.reshape(key_count, heads_here, VDIM)
        scores = jnp.einsum(
            "thd,shd->hts", query_plain, key_heads, preferred_element_type=jnp.float32
        )
        scores = (
            scores
            + jnp.einsum(
                "thd,sd->hts", query_turned, key_turned, preferred_element_type=jnp.float32
            )
        ) * score_scale
        key_positions = jnp.arange(key_count, dtype=jnp.int32)
        allowed = key_positions[None, :] <= positions[:, None]
        scores = jnp.where(allowed[None], scores, -1e30)
        new_max = jnp.maximum(row_max, jnp.max(scores, axis=-1))
        weights = jnp.exp(scores - new_max[..., None])
        row_sum = jnp.sum(weights, axis=-1)
        running = jnp.einsum(
            "hts,shd->htd",
            weights.astype(jnp.bfloat16),
            value_heads,
            preferred_element_type=jnp.float32,
        )
        return (new_max, row_sum, running)

    start_state = (
        jnp.full((heads_here, tok_rows), -1e30, jnp.float32),
        jnp.zeros((heads_here, tok_rows), jnp.float32),
        jnp.zeros((heads_here, tok_rows, VDIM), jnp.float32),
    )
    pieces = (
        lax.all_gather(kv_latent, "sp", axis=0, tiled=True),
        lax.all_gather(rope_key, "sp", axis=0, tiled=True),
    )

    def take_piece(state_in):
        key_plain, value_plain, key_turned = expand(
            pieces[0], pieces[1], latent_gain, w_key, w_value
        )
        return update(state_in, key_plain, value_plain, key_turned)

    def skip_piece(state_in):
        return state_in

    final_state = lax.cond(jnp.int32(0) <= last_row, take_piece, skip_piece, start_state)
    attended = (final_state[2] / final_state[1][..., None]).transpose(1, 0, 2)
    attended = attended.reshape(tok_rows, heads_here * VDIM).astype(jnp.bfloat16)
    chosen = attended
    product = jnp.dot(chosen, w_out, preferred_element_type=jnp.float32)
    branch = lax.psum_scatter(
        product.astype(jnp.bfloat16).astype(jnp.float32).astype(jnp.bfloat16),
        "tp",
        scatter_dimension=0,
        tiled=True,
    ).astype(jnp.float32)
    updated = (residual.astype(jnp.float32) + rms_scale(branch, post_gain)).astype(jnp.bfloat16)
    moe_in = rms_scale(updated.astype(jnp.float32), moe_gain).astype(jnp.bfloat16)
    token_count = routes.shape[0]
    experts = lax.axis_size("sp")
    capacity = max(2, 3 * token_count // experts)
    onehot = (routes[:, :, None] == jnp.arange(experts, dtype=jnp.int32)[None, None, :]).astype(
        jnp.int32
    )
    flat_hits = onehot.reshape(token_count * 2, experts)
    order_in = jnp.cumsum(flat_hits, axis=0) - flat_hits
    slot_ids = jnp.sum(
        (order_in + jnp.arange(experts, dtype=jnp.int32)[None, :] * capacity) * flat_hits, axis=1
    )
    placing = slot_ids[:, None] == jnp.arange(experts * capacity, dtype=jnp.int32)[None, :]
    placing = placing.astype(jnp.bfloat16).reshape(token_count, 2, experts * capacity)
    sending = jnp.einsum("tks,td->sd", placing, moe_in, preferred_element_type=jnp.float32).astype(
        jnp.bfloat16
    )
    received = lax.all_to_all(sending, "sp", split_axis=0, concat_axis=0, tiled=True)
    span_rows = lax.all_gather(received, "tp", axis=0, tiled=True)
    gate_pre = jnp.dot(span_rows, w_gate[0], preferred_element_type=jnp.float32)
    up_proj = jnp.dot(span_rows, w_up[0], preferred_element_type=jnp.float32)
    hidden_rows = (jax.nn.silu(gate_pre) * up_proj).astype(jnp.bfloat16)
    chosen = hidden_rows
    product = jnp.dot(chosen, w_down[0], preferred_element_type=jnp.float32)
    expert_out = lax.psum_scatter(
        product.astype(jnp.bfloat16).astype(jnp.float32).astype(jnp.bfloat16),
        "tp",
        scatter_dimension=0,
        tiled=True,
    )
    returned = lax.all_to_all(expert_out, "sp", split_axis=0, concat_axis=0, tiled=True)
    gathered_back = jnp.einsum("tks,sd->tkd", placing, returned, preferred_element_type=jnp.float32)
    weighted = jnp.sum(gathered_back * route_weight[:, :, None], axis=1)
    return (updated.astype(jnp.float32) + weighted).astype(jnp.bfloat16)


def solution(mesh):
    placed = (
        P(("grp", "sp", "tp"), None),
        P(("grp", "sp"), "tp"),
        P(("grp", "sp"), "tp"),
        P(("grp", "sp"), None),
        P(("grp", "sp"), None),
        P(),
        P(None, "tp"),
        P(None, "tp"),
        P("tp", None),
        P(),
        P(("grp", "sp", "tp"), None),
        P(("grp", "sp", "tp"), None),
        P(),
        P("sp", None, "tp"),
        P("sp", None, "tp"),
        P("sp", "tp", None),
    )
    return jax.shard_map(
        body, mesh=mesh, in_specs=placed, out_specs=P(("grp", "sp", "tp"), None), check_vma=False
    )
```

profile of v0, /device:TPU:0, one launch (start us, length us, event | category | flops | bytes accessed | tf_op | source)
XLA Modules:
  0.0 215.7 jit_solution(12267878147756269615)
XLA Ops:
  6.5 0.0 copy-start
  6.5 0.0 reduce-scatter.3.cloned.1.call-start
  6.6 1.0 copy.40
  7.6 15.3 %all_gather.10 = bf16[1024,64]{0,1:T(8,128)(2,1)S(1)} all-gather(bf16[256,64]{0,1:T(8,128)(2,1)} %param.22), channel_id=1, replica_groups=mesh['grp'=2,'sp'=4,'tp'=4] {'sp'}, dimensions={0}, use_global_device_ids=true | all-gather | bytes 163840 | tf_op jit(solution)/shard_map/all_gather | solution.py:119
  22.9 16.2 %all_gather.9 = bf16[1024,256]{1,0:T(8,128)(2,1)S(1)} all-gather(bf16[256,256]{1,0:T(8,128)(2,1)} %param.21), channel_id=1, replica_groups=mesh['grp'=2,'sp'=4,'tp'=4] {'sp'}, dimensions={0}, use_global_device_ids=true | all-gather | bytes 655360 | tf_op jit(solution)/shard_map/all_gather | solution.py:118
  39.1 0.2 multiply_cosine_fusion.1
  39.3 4.9 %conditional.1 = (f32[2,256]{1,0:T(2,128)S(1)}, f32[2,256,128]{1,2,0:T(8,128)S(1)}) conditional(s32[]{:T(128)} %convert_element_type.105, () %tuple.13, (s32[]{:T(128)}, s32[256]{0:T(256)S(1)}, bf16[1024,256]{1,0:T(8,128)(2,1)S(1)}, f32[256]{0:T(256)}, bf16[256,256]{1,0:T(8,128)(2,1)}, /*index=5*/bf16[256,256]{1,0:T(8,128)(2,1)}, ...), branch_computations={%region_0.0_spmd, %region_1.5_spmd} | conditional | flops 612468544 | bytes 17417576 | solution.py:131
  39.3 0.0 copy-start.7
  39.4 0.0 copy-start.8
  39.4 0.0 copy-start.2
  39.4 0.2 fusion.4
  39.6 0.2 iota_compare_fusion
  39.9 0.6 fusion.17
  40.4 1.4 convolution_convert_fusion
  41.8 0.0 copy-done.7
  41.8 0.0 copy-done.8
  41.9 0.5 convolution_convert_fusion.1
  42.4 0.0 copy-done.2
  42.4 0.5 fusion.20
  42.9 0.6 fusion.58
  43.4 0.5 fusion.7
  43.9 0.3 fusion.3
  44.2 0.0 copy-start.6
  44.2 0.0 copy-start.1
  44.2 0.0 copy-start.3
  44.3 0.0 copy-start.4
  44.3 0.0 copy-done
  44.3 1.5 convolution_convert_fusion.2
  45.8 0.0 reduce-scatter.3.cloned.1.call-update
  45.8 0.0 all-gather.2.cloned.1.call-start
  45.8 0.0 copy-done.6
  45.9 0.1 copy.42
  46.0 0.1 eq.54
  46.1 0.1 fusion.55
  46.2 0.2 reduce_window_sum.11
  46.4 0.2 select_reduce_fusion
  46.5 0.1 eq.58
  46.7 0.1 copy.43
  46.8 0.1 convert_reduce_fusion
  46.9 24.3 %reduce-scatter.3.cloned.1.call-done = bf16[64,2048]{1,0:T(8,128)(2,1)} async-done(((bf16[256,2048]{1,0:T(8,128)(2,1)}), bf16[64,2048]{1,0:T(8,128)(2,1)}) %reduce-scatter.3.cloned.1.call-update) | async-done | bytes 262160 | tf_op jit(solution)/shard_map/reduce_scatter | solution.py:136
  71.2 1.1 fusion.40
  72.3 0.0 copy-done.1
  72.3 0.0 copy-done.3
  72.3 1.2 fusion.44
  73.6 0.0 copy-done.4
  73.6 0.4 convolution_convert_fusion.3
  74.0 24.4 %all_to_all.24 = bf16[4,48,2048]{2,1,0:T(8,128)(2,1)} all-to-all(bf16[4,48,2048]{2,1,0:T(8,128)(2,1)S(1)} %bitcast.63), channel_id=1, replica_groups=mesh['grp'=2,'sp'=4,'tp'=4] {'sp'}, dimensions={0} | all-to-all | bytes 1572864 | tf_op jit(solution)/shard_map/all_to_all | solution.py:160
  98.5 0.0 all-gather.2.cloned.1.call-update
  98.5 0.0 reduce-scatter.5.cloned.1.call-start
  98.5 26.7 %all-gather.2.cloned.1.call-done = bf16[768,2048]{1,0:T(8,128)(2,1)} async-done(((bf16[192,2048]{1,0:T(8,128)(2,1)}), bf16[768,2048]{1,0:T(8,128)(2,1)}) %all-gather.2.cloned.1.call-update) | async-done | bytes 3145744 | tf_op jit(solution)/shard_map/all_gather | solution.py:161
  125.3 8.0 %fusion.28 = f32[768,896]{1,0:T(8,128)} fusion(bf16[768,2048]{1,0:T(8,128)(2,1)} %all-gather.2.cloned.1.call-done, bf16[1,2048,896]{2,1,0:T(8,128)(2,1)} %param.32), kind=kOutput, calls=%fused_computation.40 | convolution fusion | flops 2818572288 | bytes 9568256 | tf_op jit(solution)/shard_map/dot_general | solution.py:163
  133.3 12.2 %fusion.32 = bf16[768,2048]{1,0:T(8,128)(2,1)} fusion(bf16[1,896,2048]{2,1,0:T(8,128)(2,1)} %param.33, f32[768,896]{1,0:T(8,128)} %fusion.28, bf16[768,2048]{1,0:T(8,128)(2,1)} %all-gather.2.cloned.1.call-done, bf16[1,2048,896]{2,1,0:T(8,128)(2,1)} %param.31), kind=kOutput, calls=%fused_computation.44 | convolution fusion | flops 5642846208 | bytes 16384000 | tf_op jit(solution)/shard_map/dot_general | solution.py:166
  145.4 0.0 copy-start.5
  145.4 0.0 reduce-scatter.5.cloned.1.call-update
  145.5 38.1 %reduce-scatter.5.cloned.1.call-done = bf16[192,2048]{1,0:T(8,128)(2,1)} async-done(((bf16[768,2048]{1,0:T(8,128)(2,1)}), bf16[192,2048]{1,0:T(8,128)(2,1)}) %reduce-scatter.5.cloned.1.call-update) | async-done | bytes 786448 | tf_op jit(solution)/shard_map/reduce_scatter | solution.py:167
  183.5 24.5 %all_to_all.25 = bf16[4,48,2048]{2,1,0:T(8,128)(2,1)S(1)} all-to-all(bf16[4,48,2048]{2,1,0:T(8,128)(2,1)} %bitcast.64), channel_id=1, replica_groups=mesh['grp'=2,'sp'=4,'tp'=4] {'sp'}, dimensions={0} | all-to-all | bytes 1572864 | tf_op jit(solution)/shard_map/all_to_all | solution.py:173
  208.1 0.0 copy-done.5
  208.1 0.4 fusion.37
  208.4 0.8 fusion.47
  (15 shorter events, 0.1 us)
Async XLA Ops:
  6.5 37.8 %copy-start = (bf16[256,2048]{1,0:T(8,128)(2,1)S(1)}, bf16[256,2048]{1,0:T(8,128)(2,1)}, u32[]{:S(2)}) copy-start(bf16[256,2048]{1,0:T(8,128)(2,1)} %param.26) | copy-start | bytes 3145732
  6.5 64.6 %reduce-scatter.3.cloned.1.call-start = ((), (), s32[]{:S(2)}) async-start(), calls=%async_computation.4 | async-start | bytes 1310720 | tf_op jit(solution)/shard_map/reduce_scatter | solution.py:136
  39.3 2.5 %copy-start.7 = (bf16[256,256]{1,0:T(8,128)(2,1)S(1)}, bf16[256,256]{1,0:T(8,128)(2,1)}, u32[]{:S(2)}) copy-start(bf16[256,256]{1,0:T(8,128)(2,1)} %get-tuple-element.44) | copy-start | bytes 393220 | tf_op jit(solution)/shard_map/cond
  39.4 2.5 %copy-start.8 = (f32[256]{0:T(256)S(1)}, f32[256]{0:T(256)}, u32[]{:S(2)}) copy-start(f32[256]{0:T(256)} %get-tuple-element.43) | copy-start | bytes 3076 | tf_op jit(solution)/shard_map/cond
  39.4 3.0 %copy-start.2 = (bf16[256,256]{1,0:T(8,128)(2,1)S(1)}, bf16[256,256]{1,0:T(8,128)(2,1)}, u32[]{:S(2)}) copy-start(bf16[256,256]{1,0:T(8,128)(2,1)} %get-tuple-element.45) | copy-start | bytes 393220 | tf_op jit(solution)/shard_map/cond
  44.2 1.6 copy-start.6
  44.2 28.0 %copy-start.1 = (bf16[64,2048]{1,0:T(8,128)(2,1)S(1)}, bf16[64,2048]{1,0:T(8,128)(2,1)}, u32[]{:S(2)}) copy-start(bf16[64,2048]{1,0:T(8,128)(2,1)} %param.18) | copy-start | bytes 786436
  44.2 28.0 %copy-start.3 = (f32[2048]{0:T(1024)S(1)}, f32[2048]{0:T(1024)}, u32[]{:S(2)}) copy-start(f32[2048]{0:T(1024)} %param.27) | copy-start | bytes 24580
  44.3 29.3 %copy-start.4 = (f32[2048]{0:T(1024)S(1)}, f32[2048]{0:T(1024)}, u32[]{:S(2)}) copy-start(f32[2048]{0:T(1024)} %param.30) | copy-start | bytes 24580
  45.8 79.5 %all-gather.2.cloned.1.call-start = ((), (), s32[]{:S(2)}) async-start(), calls=%async_computation.5 | async-start | bytes 3932160 | tf_op jit(solution)/shard_map/all_gather | solution.py:161
  98.5 85.1 %reduce-scatter.5.cloned.1.call-start = ((), (), s32[]{:S(2)}) async-start(), calls=%async_computation.6 | async-start | bytes 3932160 | tf_op jit(solution)/shard_map/reduce_scatter | solution.py:167
  145.4 62.6 %copy-start.5 = (f32[64,2]{0,1:T(2,128)S(1)}, f32[64,2]{0,1:T(2,128)}, u32[]{:S(2)}) copy-start(f32[64,2]{0,1:T(2,128)} %param.29) | copy-start | bytes 1540
Sparse Core Ops, SparseCore 0:
  45.9 25.1 reduce-scatter.2
  98.6 26.6 all-gather.1
  145.6 37.9 reduce-scatter.4
where the time goes:
time: 216 us
  waiting for transfers between devices  89.2 us (41%)
  blocking collectives  80.5 us (37%)
  matrix products  25.8 us (12%)
  between operations  13.3 us (6%)
  other arithmetic  5.23 us (2%)
    reduce_scatter x2, waiting for transfers between devices, body(): lax.psum_scatter(product.astype(jnp.bfloat16).astype(jnp.float32).astype(...  62.4 us
    all_gather x1, waiting for transfers between devices, body(): span_rows = lax.all_gather(received, 'tp', axis=0, tiled=True)  26.7 us
    all_to_all x1, blocking collectives, body(): lax.all_to_all(expert_out, 'sp', split_axis=0, concat_axis=0, tiled=True)  24.5 us
    all_to_all x1, blocking collectives, body(): lax.all_to_all(sending, 'sp', split_axis=0, concat_axis=0, tiled=True)  24.4 us
    all_gather x1, blocking collectives, body(): lax.all_gather(kv_latent, 'sp', axis=0, tiled=True)  16.2 us
    all_gather x1, blocking collectives, body(): lax.all_gather(rope_key, 'sp', axis=0, tiled=True)  15.3 us
    dot_general x1, matrix products, body(): product = jnp.dot(chosen, w_down[0], preferred_element_type=jnp.float32)  12.2 us
    dot_general x1, matrix products, body(): up_proj = jnp.dot(span_rows, w_up[0], preferred_element_type=jnp.float32)  8 us
  transfers between devices with their start and end apart: 3, of which 3 were waited for; matrix products, arithmetic and copies ran while one was open for 0% of the time, Pallas kernels for 0%

commit v1 on v0

--- a/solution.py
+++ b/solution.py
@@ -1,7 +1,13 @@
+import functools
+
 import jax
 import jax.numpy as jnp
 from jax import lax
+from jax.experimental import pallas as pl
+from jax.experimental.pallas import tpu as pltpu
 from jax.sharding import PartitionSpec as P
+
+MESH = pl.DeviceIdType.MESH
 
 HEADS = 8
 NOPE = 128
@@ -47,6 +53,380 @@
         jnp.bfloat16
     )
     return (key_plain, value_plain, key_turned)
+
+
+def push(source, target, send_sem, recv_sem, where):
+    return pltpu.make_async_remote_copy(
+        src_ref=source,
+        dst_ref=target,
+        send_sem=send_sem,
+        recv_sem=recv_sem,
+        device_id=where,
+        device_id_type=MESH,
+    )
+
+
+def greet(places):
+    barrier = pltpu.get_barrier_semaphore()
+    for place in places:
+        pl.semaphore_signal(barrier, inc=1, device_id=place, device_id_type=MESH)
+    pl.semaphore_wait(barrier, len(places))
+
+
+def tp_peers():
+    me = lax.axis_index("tp")
+    high, low = me // 2, me % 2
+    return me, 2 * (1 - high) + low, 2 * high + (1 - low), 2 * (1 - high) + (1 - low)
+
+
+def keys_kernel(n_sp, own_ref, all_ref, out_sem, in_sem, pass_sem, passed_sem):
+    here = lax.axis_index("sp")
+    me, _, pair, _ = tp_peers()
+    low = me % 2
+    greet([{"sp": lax.rem(here + k, n_sp)} for k in range(1, n_sp)] + [{"tp": pair}])
+
+    def outward(k):
+        there = lax.rem(here + k, n_sp)
+        return push(
+            own_ref.at[low], all_ref.at[here, low], out_sem.at[k], in_sem.at[here], {"sp": there}
+        )
+
+    def inward(k):
+        there = lax.rem(here - k + n_sp, n_sp)
+        return push(
+            own_ref.at[low], all_ref.at[there, low], out_sem.at[k], in_sem.at[there], {"sp": there}
+        )
+
+    def relay(k, half):
+        there = lax.rem(here - k + n_sp, n_sp)
+        return push(
+            all_ref.at[there, half],
+            all_ref.at[there, half],
+            pass_sem.at[k],
+            passed_sem.at[there],
+            {"tp": pair},
+        )
+
+    def begin(k, carry):
+        @pl.when(here + k < n_sp)
+        def _():
+            outward(k).start()
+
+        return carry
+
+    lax.fori_loop(1, n_sp, begin, 0)
+    all_ref[here] = own_ref[...]
+
+    def clear(k, carry):
+        @pl.when(here + k < n_sp)
+        def _():
+            all_ref[here + k] = jnp.zeros(own_ref.shape, own_ref.dtype)
+
+        return carry
+
+    lax.fori_loop(1, n_sp, clear, 0)
+
+    def forward(k, carry):
+        @pl.when(here >= k)
+        def _():
+            inward(k).wait_recv()
+            relay(k, low).start()
+
+        return carry
+
+    lax.fori_loop(1, n_sp, forward, 0)
+
+    def finish(k, carry):
+        @pl.when(here >= k)
+        def _():
+            relay(k, 1 - low).wait_recv()
+            relay(k, low).wait_send()
+
+        @pl.when(here + k < n_sp)
+        def _():
+            outward(k).wait_send()
+
+        return carry
+
+    lax.fori_loop(1, n_sp, finish, 0)
+
+
+def gather_keys(own_rows):
+    n_sp = lax.axis_size("sp")
+    rows, width = own_rows.shape
+    sems = [pltpu.SemaphoreType.DMA((n_sp,))] * 4
+    gathered = pl.pallas_call(
+        functools.partial(keys_kernel, n_sp),
+        out_shape=jax.ShapeDtypeStruct((n_sp, 2, rows // 2, width), own_rows.dtype),
+        in_specs=[pl.BlockSpec(memory_space=pltpu.VMEM)],
+        out_specs=pl.BlockSpec(memory_space=pltpu.VMEM),
+        scratch_shapes=sems,
+        compiler_params=pltpu.CompilerParams(collective_id=0, has_side_effects=True),
+        name="gather_keys",
+    )(own_rows.reshape(2, rows // 2, width))
+    return gathered.reshape(n_sp * rows, width)
+
+
+def branch_kernel(
+    pieces, part_ref, sum_ref, far_in, own_in, mixed_out, mixed_in, a_s, a_r, b_s, b_r, c_s, c_r
+):
+    me, across, pair, far = tp_peers()
+    greet([{"tp": pair}, {"tp": across}])
+
+    def far_copy(j):
+        return push(part_ref.at[far, j], far_in.at[j], a_s.at[j], a_r.at[j], {"tp": pair})
+
+    def own_copy():
+        return push(part_ref.at[pair], own_in, b_s, b_r, {"tp": pair})
+
+    def across_copy(j):
+        return push(mixed_out.at[j], mixed_in.at[j], c_s.at[j], c_r.at[j], {"tp": across})
+
+    for j in range(pieces):
+        far_copy(j).start()
+    own_copy().start()
+    for j in range(pieces):
+        far_copy(j).wait_recv()
+        total = part_ref[across, j].astype(jnp.float32) + far_in[j].astype(jnp.float32)
+        mixed_out[j] = total.astype(jnp.bfloat16)
+        across_copy(j).start()
+    own_copy().wait_recv()
+    for j in range(pieces):
+        across_copy(j).wait_recv()
+        sum_ref[j] = (
+            part_ref[me, j].astype(jnp.float32)
+            + own_in[j].astype(jnp.float32)
+            + mixed_in[j].astype(jnp.float32)
+        )
+    for j in range(pieces):
+        far_copy(j).wait_send()
+        across_copy(j).wait_send()
+    own_copy().wait_send()
+
+
+def sum_branch(product):
+    n_tp = lax.axis_size("tp")
+    rows, width = product.shape[0] // n_tp, product.shape[1]
+    pieces = max(1, rows // 16)
+    depth = rows // pieces
+    block = pltpu.VMEM((pieces, depth, width), jnp.bfloat16)
+    many = pltpu.SemaphoreType.DMA((pieces,))
+    one = pltpu.SemaphoreType.DMA
+    summed = pl.pallas_call(
+        functools.partial(branch_kernel, pieces),
+        out_shape=jax.ShapeDtypeStruct((pieces, depth, width), jnp.float32),
+        in_specs=[pl.BlockSpec(memory_space=pltpu.VMEM)],
+        out_specs=pl.BlockSpec(memory_space=pltpu.VMEM),
+        scratch_shapes=[block] * 4 + [many, many, one, one, many, many],
+        compiler_params=pltpu.CompilerParams(collective_id=1, has_side_effects=True),
+        name="sum_branch",
+    )(product.reshape(n_tp, pieces, depth, width))
+    return summed.reshape(rows, width)
+
+
+def experts_kernel(
+    n_sp,
+    send_ref,
+    gate_hbm,
+    up_hbm,
+    down_hbm,
+    back_ref,
+    got,
+    part,
+    near,
+    mixed_out,
+    mixed_in,
+    done,
+    gate,
+    up,
+    down,
+    w_sem,
+    l_sem,
+    z_s,
+    z_r,
+    x_s,
+    x_r,
+    p_s,
+    p_r,
+    q_s,
+    q_r,
+    n_s,
+    n_r,
+    m_s,
+    m_r,
+    b_s,
+    b_r,
+):
+    here = lax.axis_index("sp")
+    _, across, pair, _ = tp_peers()
+    weights = [
+        pltpu.make_async_copy(source, target, w_sem.at[i])
+        for i, (source, target) in enumerate([(gate_hbm, gate), (up_hbm, up), (down_hbm, down)])
+    ]
+    own_copy = pltpu.make_async_copy(send_ref.at[here], got.at[here, 0], l_sem)
+    own_copy.start()
+    for copy in weights:
+        copy.start()
+    greet(
+        [{"sp": lax.rem(here + k, n_sp)} for k in range(1, n_sp)] + [{"tp": pair}, {"tp": across}]
+    )
+
+    def source_of(k):
+        return lax.rem(here - k + n_sp, n_sp)
+
+    def sp_out(k):
+        there = lax.rem(here + k, n_sp)
+        return push(send_ref.at[there], got.at[here, 0], z_s.at[k], z_r.at[here], {"sp": there})
+
+    def sp_in(k):
+        there = source_of(k)
+        return push(send_ref.at[there], got.at[there, 0], z_s.at[k], z_r.at[there], {"sp": there})
+
+    def spread_across(k):
+        s = source_of(k)
+        return push(got.at[s, 0], got.at[s, 1], x_s.at[k], x_r.at[k], {"tp": across})
+
+    def spread_pair(k):
+        s = source_of(k)
+        return push(got.at[s, 0], got.at[s, 2], p_s.at[k], p_r.at[k], {"tp": pair})
+
+    def spread_last(k):
+        s = source_of(k)
+        return push(got.at[s, 1], got.at[s, 3], q_s.at[k], q_r.at[k], {"tp": pair})
+
+    def near_copy(k):
+        return push(part.at[k, pl.ds(2, 2)], near.at[k], n_s.at[k], n_r.at[k], {"tp": pair})
+
+    def mixed_copy(k):
+        return push(mixed_out.at[k], mixed_in.at[k], m_s.at[k], m_r.at[k], {"tp": across})
+
+    def back_out(k):
+        s = source_of(k)
+        return push(done.at[k], back_ref.at[here], b_s.at[k], b_r.at[here], {"sp": s})
+
+    def back_in(k):
+        s = lax.rem(here + k, n_sp)
+        return push(done.at[k], back_ref.at[s], b_s.at[k], b_r.at[s], {"sp": s})
+
+    def begin(k, carry):
+        sp_out(k).start()
+        return carry
+
+    lax.fori_loop(1, n_sp, begin, 0)
+    own_copy.wait()
+    spread_across(0).start()
+    spread_pair(0).start()
+
+    def step(k, carry):
+        @pl.when(k + 1 < n_sp)
+        def _():
+            sp_in(k + 1).wait_recv()
+            spread_across(k + 1).start()
+            spread_pair(k + 1).start()
+
+        @pl.when(k < n_sp)
+        def _():
+            spread_across(k).wait_recv()
+            spread_last(k).start()
+
+        @pl.when(jnp.logical_and(k >= 1, k <= n_sp))
+        def _():
+            near_copy(k - 1).wait_recv()
+            total = part[k - 1, 1].astype(jnp.float32) + near[k - 1, 1].astype(jnp.float32)
+            mixed_out[k - 1] = total.astype(jnp.bfloat16)
+            mixed_copy(k - 1).start()
+
+        @pl.when(k == 0)
+        def _():
+            for copy in weights:
+                copy.wait()
+
+        @pl.when(k < n_sp)
+        def _():
+            spread_pair(k).wait_recv()
+            spread_last(k).wait_recv()
+            block = got[source_of(k)]
+            rows = block.reshape(block.shape[0] * block.shape[1], block.shape[2])
+            gate_pre = jnp.dot(rows, gate[...], preferred_element_type=jnp.float32)
+            up_proj = jnp.dot(rows, up[...], preferred_element_type=jnp.float32)
+            hidden = (gate_pre / (1.0 + jnp.exp(-gate_pre)) * up_proj).astype(jnp.bfloat16)
+            product = jnp.dot(hidden, down[...], preferred_element_type=jnp.float32)
+            part[k] = product.astype(jnp.bfloat16).reshape(block.shape)
+            near_copy(k).start()
+
+        def summed(j):
+            mixed_copy(j).wait_recv()
+            return (
+                part[j, 0].astype(jnp.float32)
+                + near[j, 0].astype(jnp.float32)
+                + mixed_in[j].astype(jnp.float32)
+            ).astype(jnp.bfloat16)
+
+        @pl.when(k == 2)
+        def _():
+            back_ref[here] = summed(0)
+
+        @pl.when(k > 2)
+        def _():
+            done[k - 2] = summed(k - 2)
+            back_out(k - 2).start()
+
+        return carry
+
+    lax.fori_loop(0, n_sp + 2, step, 0)
+
+    def finish(k, carry):
+        spread_across(k).wait_send()
+        spread_pair(k).wait_send()
+        spread_last(k).wait_send()
+        near_copy(k).wait_send()
+        mixed_copy(k).wait_send()
+
+        @pl.when(k >= 1)
+        def _():
+            sp_out(k).wait_send()
+            back_out(k).wait_send()
+            back_in(k).wait_recv()
+
+        return carry
+
+    lax.fori_loop(0, n_sp, finish, 0)
+
+
+def run_experts(sending, w_gate, w_up, w_down):
+    n_sp, depth, width = sending.shape
+    hidden = w_gate.shape[1]
+    half = jnp.bfloat16
+    block = pltpu.VMEM((n_sp, depth, width), half)
+    sems = pltpu.SemaphoreType.DMA((n_sp,))
+    vmem = pl.BlockSpec(memory_space=pltpu.VMEM)
+    hbm = pl.BlockSpec(memory_space=pl.ANY)
+    flops = 6 * n_sp * 4 * depth * width * hidden
+    return pl.pallas_call(
+        functools.partial(experts_kernel, n_sp),
+        out_shape=jax.ShapeDtypeStruct(sending.shape, half),
+        in_specs=[vmem, hbm, hbm, hbm],
+        out_specs=vmem,
+        scratch_shapes=[
+            pltpu.VMEM((n_sp, 4, depth, width), half),
+            pltpu.VMEM((n_sp, 4, depth, width), half),
+            pltpu.VMEM((n_sp, 2, depth, width), half),
+            block,
+            block,
+            block,
+            pltpu.VMEM((width, hidden), half),
+            pltpu.VMEM((width, hidden), half),
+            pltpu.VMEM((hidden, width), half),
+            pltpu.SemaphoreType.DMA((3,)),
+            pltpu.SemaphoreType.DMA,
+        ]
+        + [sems] * 14,
+        compiler_params=pltpu.CompilerParams(
+            collective_id=2, has_side_effects=True, vmem_limit_bytes=60 * 2**20
+        ),
+        cost_estimate=pl.CostEstimate(flops=flops, bytes_accessed=flops // 64, transcendentals=0),
+        name="run_experts",
+    )(sending, w_gate, w_up, w_down)
 
 
 def body(
@@ -70,7 +450,6 @@
     tok_rows = query_nope.shape[0]
     heads_here = HEADS // lax.axis_size("tp")
     first_row = lax.axis_index("sp") * tok_rows
-    last_row = first_row + tok_rows - 1
     positions = first_row + jnp.arange(tok_rows, dtype=jnp.int32)
     cosine_table, sine_table = tables(positions, ROPE)
     query_plain = query_nope.reshape(tok_rows, heads_here, NOPE)
@@ -114,10 +493,9 @@
         jnp.zeros((heads_here, tok_rows), jnp.float32),
         jnp.zeros((heads_here, tok_rows, VDIM), jnp.float32),
     )
-    pieces = (
-        lax.all_gather(kv_latent, "sp", axis=0, tiled=True),
-        lax.all_gather(rope_key, "sp", axis=0, tiled=True),
-    )
+    rank = kv_latent.shape[1]
+    gathered = gather_keys(jnp.concatenate([kv_latent, rope_key], axis=1))
+    pieces = (gathered[:, :rank], gathered[:, rank:])
 
     def take_piece(state_in):
         key_plain, value_plain, key_turned = expand(
@@ -125,25 +503,18 @@
         )
         return update(state_in, key_plain, value_plain, key_turned)
 
-    def skip_piece(state_in):
-        return state_in
-
-    final_state = lax.cond(jnp.int32(0) <= last_row, take_piece, skip_piece, start_state)
+    final_state = take_piece(start_state)
     attended = (final_state[2] / final_state[1][..., None]).transpose(1, 0, 2)
     attended = attended.reshape(tok_rows, heads_here * VDIM).astype(jnp.bfloat16)
     chosen = attended
     product = jnp.dot(chosen, w_out, preferred_element_type=jnp.float32)
-    branch = lax.psum_scatter(
-        product.astype(jnp.bfloat16).astype(jnp.float32).astype(jnp.bfloat16),
-        "tp",
-        scatter_dimension=0,
-        tiled=True,
-    ).astype(jnp.float32)
+    branch = sum_branch(product.astype(jnp.bfloat16))
     updated = (residual.astype(jnp.float32) + rms_scale(branch, post_gain)).astype(jnp.bfloat16)
     moe_in = rms_scale(updated.astype(jnp.float32), moe_gain).astype(jnp.bfloat16)
     token_count = routes.shape[0]
     experts = lax.axis_size("sp")
     capacity = max(2, 3 * token_count // experts)
+    capacity = -(-capacity // 16) * 16
     onehot = (routes[:, :, None] == jnp.arange(experts, dtype=jnp.int32)[None, None, :]).astype(
         jnp.int32
     )
@@ -157,20 +528,9 @@
     sending = jnp.einsum("tks,td->sd", placing, moe_in, preferred_element_type=jnp.float32).astype(
         jnp.bfloat16
     )
-    received = lax.all_to_all(sending, "sp", split_axis=0, concat_axis=0, tiled=True)
-    span_rows = lax.all_gather(received, "tp", axis=0, tiled=True)
-    gate_pre = jnp.dot(span_rows, w_gate[0], preferred_element_type=jnp.float32)
-    up_proj = jnp.dot(span_rows, w_up[0], preferred_element_type=jnp.float32)
-    hidden_rows = (jax.nn.silu(gate_pre) * up_proj).astype(jnp.bfloat16)
-    chosen = hidden_rows
-    product = jnp.dot(chosen, w_down[0], preferred_element_type=jnp.float32)
-    expert_out = lax.psum_scatter(
-        product.astype(jnp.bfloat16).astype(jnp.float32).astype(jnp.bfloat16),
-        "tp",
-        scatter_dimension=0,
-        tiled=True,
-    )
-    returned = lax.all_to_all(expert_out, "sp", split_axis=0, concat_axis=0, tiled=True)
+    sending = sending.reshape(experts, capacity, sending.shape[1])
+    returned = run_experts(sending, w_gate[0], w_up[0], w_down[0])
+    returned = returned.reshape(experts * capacity, returned.shape[2])
     gathered_back = jnp.einsum("tks,sd->tkd", placing, returned, preferred_element_type=jnp.float32)
     weighted = jnp.sum(gathered_back * route_weight[:, :, None], axis=1)
     return (updated.astype(jnp.float32) + weighted).astype(jnp.bfloat16)

time: 216 us -> 112 us (0.52)
  Pallas kernels: 0 us -> 92.4 us
  waiting for transfers between devices: 89.2 us -> 0 us
  blocking collectives: 80.5 us -> 0 us
  matrix products: 25.8 us -> 7.86 us
  between operations: 13.3 us -> 0.32 us
  other arithmetic: 5.23 us -> 8.04 us
    pallas_call x0 -> x3, Pallas kernels: none -> 92.4 us  [the longest x1 67 us: run_experts(): pl.pallas_call(functools.partial(experts_kernel, n_sp), out_shape=jax.Sha...]
    reduce_scatter x2 -> x0, waiting for transfers between devices: 62.4 us -> none  [body(): lax.psum_scatter(product.astype(jnp.bfloat16).astype(jnp.float32).astype(...]
    all_to_all x2 -> x0, blocking collectives: 49 us -> none  [the longest x1 24.5 us: body(): lax.all_to_all(expert_out, 'sp', split_axis=0, concat_axis=0, tiled=True)]
    all_gather x2 -> x0, blocking collectives: 31.5 us -> none  [the longest x1 16.2 us: body(): lax.all_gather(kv_latent, 'sp', axis=0, tiled=True)]
    all_gather x1 -> x0, waiting for transfers between devices: 26.7 us -> none  [body(): span_rows = lax.all_gather(received, 'tp', axis=0, tiled=True)]
    dot_general x2 -> x1, matrix products: 20.2 us -> 0.52 us  [update(): jnp.einsum('hts,shd->htd', weights.astype(jnp.bfloat16), value_heads, pre...]
  transfers between devices with their start and end apart: 3 -> 0, of which waited for: 3 -> 0; matrix products, arithmetic and copies ran while one was open for 0% -> 0% of each run, Pallas kernels for 0% -> 0%
where the time goes in v1:
time: 112 us; the launch traced here: 111 us
  Pallas kernels  92.4 us (82%)
  other arithmetic  8.04 us (7%)
  matrix products  7.86 us (7%)
  local copies, waits for them, and re-layouts  2.48 us (2%)
    pallas_call x1, Pallas kernels, run_experts(): pl.pallas_call(functools.partial(experts_kernel, n_sp), out_shape=jax.Sha...  67 us
    pallas_call x1, Pallas kernels, gather_keys(): pl.pallas_call(functools.partial(keys_kernel, n_sp), out_shape=jax.ShapeD...  13.3 us
    pallas_call x1, Pallas kernels, sum_branch(): pl.pallas_call(functools.partial(branch_kernel, pieces), out_shape=jax.Sh...  12 us
    reduce_sum x3, other arithmetic, rms_scale(): mean_square = jnp.mean(inputs * inputs, axis=-1, keepdims=True)  3.83 us

profile of v1, /device:TPU:0, one launch (start us, length us, event | category | flops | bytes accessed | tf_op | source)
XLA Modules:
  0.0 111.0 jit_solution(16107305788404895655)
XLA Ops:
  0.0 0.0 copy-start
  0.0 0.0 copy-start.8
  0.0 0.0 copy-start.10
  0.0 0.0 copy-start.4
  0.0 0.9 copy.39
  0.9 0.1 eq.54
  1.0 0.1 fusion.44
  1.1 0.2 reduce_window_sum.11
  1.3 0.2 select_reduce_fusion
  1.5 0.1 eq.58
  1.6 0.1 copy.40
  1.7 0.1 convert_reduce_fusion
  1.8 0.9 copy.33
  2.7 1.6 %pad_maximum_fusion = bf16[256,320]{1,0:T(8,128)(2,1)} fusion(bf16[256,64]{1,0:T(8,128)(2,1)S(1)} %copy.33, bf16[256,256]{1,0:T(8,128)(2,1)} %param.19), kind=kLoop, calls=%fused_computation.36 | loop fusion | flops 327680 | bytes 327680 | tf_op jit(solution)/shard_map/concatenate | solution.py:497
  4.3 13.3 %gather_keys.1 = bf16[4,2,128,320]{3,2,1,0:T(8,128)(2,1)} custom-call(bf16[2,128,320]{2,1,0:T(8,128)(2,1)} %bitcast.68), custom_call_target="tpu_custom_call" | custom-call | tf_op jit(solution)/shard_map/gather_keys/pallas_call | solution.py:158
  17.6 0.0 copy-start.1
  17.6 0.0 copy-start.9
  17.6 1.3 %fusion.7 = f32[1024]{0:T(1024)S(1)} fusion(bf16[1024,320]{1,0:T(8,128)(2,1)} %bitcast.62), kind=kLoop, calls=%fused_computation.17 | loop fusion | flops 785408 | bytes 528384 | tf_op jit(solution)/shard_map/reduce_sum | solution.py:23
  19.0 0.0 copy-done.8
  19.0 0.0 copy-done.10
  19.0 1.5 %convolution_convert_fusion.2 = bf16[1024,256]{0,1:T(8,128)(2,1)S(1)} fusion(bf16[256,256]{1,0:T(8,128)(2,1)S(1)} %copy-done.8, f32[256]{0:T(256)S(1)} %copy-done.10, f32[1024]{0:T(1024)S(1)} %add_rsqrt_fusion, bf16[1024,320]{1,0:T(8,128)(2,1)} %bitcast.63), kind=kOutput, calls=%fused_computation.11 | convolution fusion | flops 135528448 | bytes 1184768 | tf_op jit(solution)/shard_map/dot_general | solution.py:49
  20.5 0.0 copy-start.3
  20.5 0.0 copy-done.4
  20.5 0.1 copy.37
  20.7 0.2 multiply_cosine_fusion.1
  20.9 0.0 copy-done.1
  21.0 0.1 copy.44
  21.1 0.6 fusion.27
  21.7 0.0 copy-done.9
  21.7 0.5 convolution_convert_fusion.3
  22.2 0.0 copy-done.3
  22.2 0.5 fusion.30
  22.7 0.2 iota_compare_fusion
  22.9 0.6 fusion.48
  23.4 0.3 fusion.2
  23.7 0.5 fusion.6
  24.3 0.0 copy-done
  24.3 0.0 copy-start.2
  24.3 0.0 copy-start.5
  24.3 1.5 %convolution_convert_fusion = bf16[256,2048]{1,0:T(8,128)(2,1)} fusion(bf16[256,256]{0,1:T(8,128)(2,1)S(1)} %bitcast.71, bf16[256,2048]{1,0:T(8,128)(2,1)S(1)} %copy-done), kind=kOutput, calls=%fused_computation | convolution fusion | flops 268959744 | bytes 2228224 | tf_op jit(solution)/shard_map/dot_general | solution.py:510
  25.8 0.0 copy-start.6
  25.8 12.0 %sum_branch.1 = f32[4,16,2048]{2,1,0:T(8,128)} custom-call(bf16[4,4,16,2048]{3,2,1,0:T(8,128)(2,1)} %bitcast.61), custom_call_target="tpu_custom_call" | custom-call | tf_op jit(solution)/shard_map/sum_branch/pallas_call | solution.py:215
  37.8 1.2 %multiply_reduce_fusion = f32[4,16]{1,0:T(4,128)S(1)} fusion(f32[4,16,2048]{2,1,0:T(8,128)} %sum_branch.1), kind=kLoop, calls=%fused_computation.33 | loop fusion | flops 262080 | bytes 524544 | tf_op jit(solution)/shard_map/reduce_sum | solution.py:23
  38.9 0.1 rsqrt.29
  39.0 0.0 copy-done.2
  39.0 0.0 copy-done.5
  39.0 1.3 %fusion.12 = (f32[64]{0:T(128)S(1)}, bf16[64,2048]{1,0:T(8,128)(2,1)S(1)}) fusion(f32[2048]{0:T(1024)S(1)} %copy-done.5, f32[64]{0:T(128)S(1)} %rsqrt.29, f32[4,16,2048]{2,1,0:T(8,128)} %sum_branch.1, bf16[64,2048]{1,0:T(8,128)(2,1)S(1)} %copy-done.2), kind=kLoop, calls=%fused_computation.25 | loop fusion | flops 1048512 | bytes 1057280 | tf_op jit(solution)/shard_map/reduce_sum | solution.py:23
  40.4 0.0 copy-done.6
  40.4 1.3 %convolution_convert_fusion.1 = bf16[192,2048]{1,0:T(8,128)(2,1)} fusion(bf16[64,192]{1,0:T(8,128)(2,1)S(1)} %convert_reduce_fusion, bf16[64,2048]{1,0:T(8,128)(2,1)S(1)} %get-tuple-element.6, f32[2048]{0:T(1024)S(1)} %copy-done.6, f32[64]{0:T(128)S(1)} %add_rsqrt_fusion.2), kind=kOutput, calls=%fused_computation.1 | convolution fusion | flops 50855936 | bytes 1081600 | tf_op jit(solution)/shard_map/tks,td->sd/dot_general | solution.py:528
  41.7 0.0 copy-start.7
  41.7 67.0 %run_experts.1 = bf16[4,48,2048]{2,1,0:T(8,128)(2,1)} custom-call(bf16[4,48,2048]{2,1,0:T(8,128)(2,1)} %bitcast.67, bf16[2048,896]{1,0:T(8,128)(2,1)} %bitcast.73, bf16[2048,896]{1,0:T(8,128)(2,1)} %bitcast.74, bf16[896,2048]{1,0:T(8,128)(2,1)} %bitcast.75), custom_call_target="tpu_custom_call" | custom-call | flops 8455716864 | bytes 132120576 | tf_op jit(solution)/shard_map/run_experts/pallas_call | solution.py:405
  108.8 0.0 copy-done.7
  108.8 1.5 %fusion.4 = f32[64,2048]{1,0:T(8,128)S(1)} fusion(bf16[192,2048,1]{1,0,2:T(8,128)(2,1)} %bitcast.66, f32[64,2]{0,1:T(2,128)S(1)} %copy-done.7, s32[64,2]{0,1:T(2,128)S(1)} %copy.40), kind=kOutput, calls=%fused_computation.13 | convolution fusion | flops 101081088 | bytes 1311744 | tf_op jit(solution)/shard_map/tks,sd->tkd/dot_general | solution.py:534
  110.3 0.8 fusion.15
  (11 shorter events, 0.1 us)
Async XLA Ops:
  0.0 24.3 %copy-start = (bf16[256,2048]{1,0:T(8,128)(2,1)S(1)}, bf16[256,2048]{1,0:T(8,128)(2,1)}, u32[]{:S(2)}) copy-start(bf16[256,2048]{1,0:T(8,128)(2,1)} %param.24) | copy-start | bytes 3145732
  0.0 19.0 %copy-start.8 = (bf16[256,256]{1,0:T(8,128)(2,1)S(1)}, bf16[256,256]{1,0:T(8,128)(2,1)}, u32[]{:S(2)}) copy-start(bf16[256,256]{1,0:T(8,128)(2,1)} %param.23) | copy-start | bytes 393220
  0.0 19.0 %copy-start.10 = (f32[256]{0:T(256)S(1)}, f32[256]{0:T(256)}, u32[]{:S(2)}) copy-start(f32[256]{0:T(256)} %param.21) | copy-start | bytes 3076
  0.0 20.5 %copy-start.4 = (bf16[256,128]{1,0:T(8,128)(2,1)S(1)}, bf16[256,128]{1,0:T(8,128)(2,1)}, u32[]{:S(2)}) copy-start(bf16[256,128]{1,0:T(8,128)(2,1)} %param.18) | copy-start | bytes 196612
  17.6 3.3 %copy-start.1 = (bf16[4,2,128,320]{3,2,1,0:T(8,128)(2,1)S(1)}, bf16[4,2,128,320]{3,2,1,0:T(8,128)(2,1)}, u32[]{:S(2)}) copy-start(bf16[4,2,128,320]{3,2,1,0:T(8,128)(2,1)} %gather_keys.1) | copy-start | bytes 1966084
  17.6 4.1 %copy-start.9 = (bf16[256,256]{1,0:T(8,128)(2,1)S(1)}, bf16[256,256]{1,0:T(8,128)(2,1)}, u32[]{:S(2)}) copy-start(bf16[256,256]{1,0:T(8,128)(2,1)} %param.22) | copy-start | bytes 393220
  20.5 1.7 %copy-start.3 = (bf16[256,256]{1,0:T(8,128)(2,1)S(1)}, bf16[256,256]{1,0:T(8,128)(2,1)}, u32[]{:S(2)}) copy-start(bf16[256,256]{1,0:T(8,128)(2,1)} %param.17) | copy-start | bytes 393220
  24.3 14.8 %copy-start.2 = (bf16[64,2048]{1,0:T(8,128)(2,1)S(1)}, bf16[64,2048]{1,0:T(8,128)(2,1)}, u32[]{:S(2)}) copy-start(bf16[64,2048]{1,0:T(8,128)(2,1)} %param.16) | copy-start | bytes 786436
  24.3 14.7 %copy-start.5 = (f32[2048]{0:T(1024)S(1)}, f32[2048]{0:T(1024)}, u32[]{:S(2)}) copy-start(f32[2048]{0:T(1024)} %param.25) | copy-start | bytes 24580
  25.8 14.6 %copy-start.6 = (f32[2048]{0:T(1024)S(1)}, f32[2048]{0:T(1024)}, u32[]{:S(2)}) copy-start(f32[2048]{0:T(1024)} %param.28) | copy-start | bytes 24580
  41.7 67.1 %copy-start.7 = (f32[64,2]{0,1:T(2,128)S(1)}, f32[64,2]{0,1:T(2,128)}, u32[]{:S(2)}) copy-start(f32[64,2]{0,1:T(2,128)} %param.27) | copy-start | bytes 1540
